TPU v7x, 128 devices: a whole 4x4x4 slice. The times are simulated.
128 devices in a mesh: ep: 128 (over z, y, x, core).
Axes of the slice: x: 4, y: 4, z: 4, core: 2. Of those that a mesh axis runs over, the one named last changes fastest.
Arguments:
- tokens: bfloat16 [1024, 2048], P('ep'), may hold values from -6 to 6
- cache_keys: bfloat16 [1024, 1024, 128], P('ep'), may hold values from -80 to 80
- cache_values: bfloat16 [1024, 1024, 128], P('ep'), may hold values from -6 to 6
- cum_gates: float32 [1024, 1024, 2], P('ep'), may hold values from -1024 to 0, as said below
- lengths: int32 [1024], P('ep'), may hold values from 128 to 1024
- query_weight: bfloat16 [2048, 2048], replicated, may hold values from -0.125 to 0.125
- key_weight: bfloat16 [2048, 128], replicated, may hold values from -0.125 to 0.125
- value_weight: bfloat16 [2048, 128], replicated, may hold values from -0.125 to 0.125
- forget_weight: bfloat16 [2048, 2], replicated, may hold values from -0.125 to 0.125
- out_weight: bfloat16 [2048, 2048], P('ep'), may hold values from -1 to 1
- norm_gain: float32 [2, 2048], replicated, may hold values from 0.1 to 1.9
- norm_bias: float32 [2, 2048], replicated, may hold values from -1 to 1
- dense_gate_weight: bfloat16 [2048, 5632], P(None, 'ep'), may hold values from -0.125 to 0.125
- dense_up_weight: bfloat16 [2048, 5632], P(None, 'ep'), may hold values from -0.125 to 0.125
- dense_down_weight: bfloat16 [5632, 2048], P('ep'), may hold values from -0.078125 to 0.078125
- dense_scale: float32 [2048], replicated, may hold values from 0.2 to 1.5
- expert_gate_weight: bfloat16 [2048, 57344], P(None, 'ep'), may hold values from -0.125 to 0.125
- expert_up_weight: bfloat16 [2048, 57344], P(None, 'ep'), may hold values from -0.125 to 0.125
- expert_down_weight: bfloat16 [57344, 2048], P('ep'), may hold values from -0.0625 to 0.0625
- routes: int32 [1024, 2], replicated, may hold values from 0 to 7, all different within a row; in each aligned block of 8 rows (0 to 7, 8 to 15, ...) at most 3 rows name the same one
- route_weights: float32 [1024, 2], replicated, may hold values from 0.2 to 1
Outputs:
- output: bfloat16 [1024, 2048], P('ep')
Inputs may be any that keep to these rules, and one draw needn't show every extreme that they name: `routes`: each row names 2 different experts; the rows of one device (8 aligned rows) name one expert at most 3 times. `cum_gates`: non-increasing along positions.
All inputs are finite; a program needn't handle non-finite values.
Results may differ from a plain program's by a relative error of at most 0.012.
Values may be sent and summed in bfloat16 or wider, within the bound.
A program may use at most 128 MiB of HBM per device.

v0:
```python
import functools
import jax
import jax.numpy as jnp
from jax import lax
from jax.experimental import pallas as pl
from jax.experimental.pallas import tpu as pltpu
from jax.sharding import PartitionSpec as P

EXPERTS = 8
MESH = pl.DeviceIdType.MESH

residual_scale = 1.4142135
norm_eps = 1e-05


def layer_norm(values, gain_row, shift_row):
    centre = jnp.mean(values, axis=-1, keepdims=True)
    centred = values - centre
    spread = jnp.mean(centred * centred, axis=-1, keepdims=True)
    return (centred * lax.rsqrt(spread + norm_eps) * gain_row + shift_row).astype(jnp.bfloat16)


def attend(
    heads, kv_count, tokens_ref, query_weight_ref, key_weight_ref, value_weight_ref,
    forget_ref, keys_ref, values_ref, gates_ref, lengths_ref, query_ref, rows_ref, waits, parts,
):
    seqs, model = tokens_ref.shape
    width = key_weight_ref.shape[1]
    head_dim = width // kv_count
    grouped = heads // kv_count
    cache_len = keys_ref.shape[1]
    ratio_value = head_dim ** (-0.5)
    tokens = tokens_ref[...]
    wide = tokens.astype(jnp.float32)
    fresh_gate = jax.nn.log_sigmoid(
        jnp.concatenate(
            [
                jnp.sum(wide * forget_ref[j:j + 1, :].astype(jnp.float32), axis=1, keepdims=True)
                for j in range(kv_count)
            ],
            axis=1,
        )
    )
    waits["keys"]()
    fresh_key = jnp.dot(tokens, key_weight_ref[...], preferred_element_type=jnp.float32)
    fresh_key = fresh_key.astype(jnp.bfloat16).astype(jnp.float32)
    fresh_value = jnp.dot(tokens, value_weight_ref[...], preferred_element_type=jnp.float32)
    fresh_value = fresh_value.astype(jnp.bfloat16).astype(jnp.float32)
    pieces = waits["pieces"]
    piece = model // pieces
    for i in range(pieces):
        waits["query"](i)
        part = jnp.dot(
            tokens, query_weight_ref[:, i * piece:(i + 1) * piece], preferred_element_type=jnp.float32
        ).astype(jnp.bfloat16).astype(jnp.float32)
        for h in range(piece // head_dim):
            head = i * (piece // head_dim) + h
            group = head // grouped
            fields = [jnp.zeros((seqs, head_dim), jnp.float32)] * kv_count
            fields[group] = part[:, h * head_dim:(h + 1) * head_dim]
            query_ref[head * seqs:(head + 1) * seqs, :] = jnp.concatenate(fields, axis=1)
    waits["caches"]()
    positions = lax.broadcasted_iota(jnp.int32, (kv_count, cache_len), 1)
    row_group = lax.broadcasted_iota(jnp.int32, (heads, 1), 0) // grouped
    lanes = rows_ref.shape[1]
    share = head_dim // parts
    for b in range(seqs):
        length = lengths_ref[b]
        gates = gates_ref[b]
        latest = jnp.sum(jnp.where(positions == length - 1, gates, 0.0), axis=1, keepdims=True)
        offsets = jnp.where(positions < length, latest - gates, -jnp.inf)
        spread = offsets[0:1] + fresh_gate[b:b + 1, 0:1]
        spread = jnp.broadcast_to(spread, (heads, cache_len))
        for j in range(1, kv_count):
            spread = jnp.where(row_group == j, offsets[j:j + 1] + fresh_gate[b:b + 1, j:j + 1], spread)
        queries = query_ref[pl.ds(b, heads, stride=seqs), :]
        past = lax.dot_general(
            queries.astype(jnp.bfloat16), keys_ref[b], (((1,), (1,)), ((), ())),
            preferred_element_type=jnp.float32,
        )
        past = past * ratio_value + spread
        self_part = ratio_value * jnp.sum(queries * fresh_key[b:b + 1], axis=1, keepdims=True)
        highest = jnp.maximum(jnp.max(past, axis=1, keepdims=True), self_part)
        past_exp = jnp.exp(past - highest)
        own_exp = jnp.exp(self_part - highest)
        denominator = jnp.sum(past_exp, axis=1, keepdims=True) + own_exp
        past_weight = (past_exp / denominator).astype(jnp.bfloat16)
        own_weight = (own_exp / denominator).astype(jnp.bfloat16).astype(jnp.float32)
        mixed = jnp.dot(past_weight, values_ref[b], preferred_element_type=jnp.float32)
        mixed = mixed + own_weight * fresh_value[b:b + 1]
        mixed = jnp.concatenate(
            [
                mixed[j * grouped:(j + 1) * grouped, j * head_dim:(j + 1) * head_dim]
                for j in range(kv_count)
            ],
            axis=0,
        )
        for p in range(parts):
            block = mixed[:, p * share:(p + 1) * share]
            if share < lanes:
                block = jnp.concatenate([block, jnp.zeros((heads, lanes - share), jnp.float32)], axis=1)
            rows_ref[pl.ds(p * seqs + b, heads, stride=parts * seqs), :] = block


def factors_of(count):
    found = [2]
    rest = count // 2
    while rest > 1:
        step = 4 if rest % 4 == 0 else rest
        found.append(step)
        rest //= step
    return found


def orders_of(stages):
    far = list(range(1, stages))
    return [[0] + far, [0] + far[::-1]]


def step_shapes(factors, order, rows, width):
    left = list(range(len(factors)))[::-1]
    shapes = []
    for axis in order:
        left = [other for other in left if other != axis]
        lead = tuple(factors[other] for other in left)
        shapes.append(((factors[axis] - 1,) + lead + (rows, width), lead + (rows, width)))
    return shapes


def kernel(
    count, factors, orders, widths, heads,
    tokens_ref, gates_ref, lengths_ref, forget_ref, gain_ref, bias_ref, scale_ref,
    routes_ref, shares_ref, query_hbm, key_hbm, value_hbm, keys_hbm, values_hbm, out_hbm,
    gate_hbm, up_hbm, down_hbm, dense_gate_hbm, dense_up_hbm, dense_down_hbm,
    result_ref, *scratch,
):
    pool = list(scratch)
    take = lambda amount: [pool.pop(0) for _ in range(amount)]
    gate_ref, up_ref, down_ref, dense_gate_ref, dense_up_ref, dense_down_ref, load_sem = take(7)
    query_weight_ref, key_weight_ref, value_weight_ref, keys_ref, values_ref, out_weight_ref, early_sem = take(7)
    query_ref, attended_rows_ref, attended_ref, share_ref = take(4)
    mixed_ref, mixed_send, mixed_recv, rows_ref, hidden_ref, dense_ref, settled_ref = take(7)
    stages = len(factors)
    chunks = len(orders)
    exchanges = []
    for _ in range(2):
        per_chunk = []
        for c in range(chunks):
            start = take(1)[0]
            lands = take(stages)
            sums = take(stages - 1)
            per_chunk.append((start, lands, sums))
        exchanges.append((per_chunk, take(2)))
    gathered = take(chunks)
    gather_send, gather_recv = take(2)
    total_rows, model = rows_ref.shape
    seqs = tokens_ref.shape[0]

    me = lax.axis_index("ep")
    coords, strides, rest, stride = [], [], me, 1
    for factor in factors:
        coords.append(lax.rem(rest, factor))
        strides.append(stride)
        rest = rest // factor
        stride *= factor

    def partner(axis, k):
        other = lax.rem(coords[axis] + k, factors[axis])
        return other, me + (other - coords[axis]) * strides[axis]

    sources = (gate_hbm, up_hbm, down_hbm, dense_gate_hbm, dense_up_hbm, dense_down_hbm)
    targets = (gate_ref, up_ref, down_ref, dense_gate_ref, dense_up_ref, dense_down_ref)
    loads = [
        pltpu.make_async_copy(source, target, load_sem.at[i])
        for i, (source, target) in enumerate(zip(sources, targets))
    ]
    barrier = pltpu.get_barrier_semaphore()

    @pl.loop(1, count)
    def _(k):
        pl.semaphore_signal(
            barrier, inc=1, device_id=(lax.rem(me + k, count),), device_id_type=MESH
        )

    model_width = tokens_ref.shape[1]
    pieces = 4
    piece = model_width // pieces
    early = [
        pltpu.make_async_copy(source, target, early_sem.at[i])
        for i, (source, target) in enumerate(
            [(key_hbm, key_weight_ref), (value_hbm, value_weight_ref)]
            + [
                (
                    query_hbm.at[:, pl.ds(i * piece, piece)],
                    query_weight_ref.at[:, pl.ds(i * piece, piece)],
                )
                for i in range(pieces)
            ]
            + [(keys_hbm, keys_ref), (values_hbm, values_ref), (out_hbm, out_weight_ref)]
        )
    ]
    for copy in early:
        copy.start()

    def wait_all(some):
        for copy in some:
            copy.wait()

    def wait_caches():
        for load in loads:
            load.start()
        wait_all(early[2 + pieces:])

    waits = {
        "keys": lambda: wait_all(early[:2]),
        "query": lambda i: early[2 + i].wait(),
        "pieces": pieces,
        "caches": wait_caches,
    }
    kv_count = gates_ref.shape[1]
    attend(
        heads, kv_count, tokens_ref, query_weight_ref, key_weight_ref, value_weight_ref,
        forget_ref, keys_ref, values_ref, gates_ref, lengths_ref, query_ref,
        attended_rows_ref, waits, count // heads,
    )
    attended_ref[...] = attended_rows_ref[...].reshape(attended_ref.shape).astype(jnp.bfloat16)
    pl.semaphore_wait(barrier, count - 1)

    def mixed_copy(k):
        to = lax.rem(me + k, count)
        return pltpu.make_async_remote_copy(
            src_ref=attended_ref.at[to], dst_ref=mixed_ref.at[me],
            send_sem=mixed_send.at[k - 1], recv_sem=mixed_recv.at[k - 1],
            device_id=(to,), device_id_type=MESH,
        )

    @pl.loop(1, count)
    def _(k):
        mixed_copy(k).start()

    mixed_ref[me] = attended_ref[me]
    own_expert = me // (count // EXPERTS)
    row_tile = min(total_rows, 256)
    diagonal = lax.broadcasted_iota(jnp.int32, (row_tile, row_tile), 0) == lax.broadcasted_iota(
        jnp.int32, (row_tile, row_tile), 1
    )
    for i in range(total_rows // row_tile):
        at = slice(i * row_tile, (i + 1) * row_tile)
        chosen = jnp.sum(
            jnp.where(routes_ref[:, at] == own_expert, shares_ref[:, at], 0.0), axis=0, keepdims=True
        )
        share_ref[at, :] = jnp.sum(jnp.where(diagonal, chosen, 0.0), axis=1, keepdims=True)

    @pl.loop(1, count)
    def _(k):
        mixed_copy(k).wait()

    def at_axis(left, axis, index):
        return tuple(index if other == axis else slice(None) for other in left)

    def exchanger(exchange):
        per_chunk, (send_sem, recv_sem) = exchange
        current = [entry[0] for entry in per_chunk]
        left = [list(range(stages))[::-1] for _ in orders]
        flying = [None] * chunks
        finished = [None] * chunks

        def launch(c, stage):
            axis = orders[c][stage]
            copies = []
            for k in range(1, factors[axis]):
                other, device = partner(axis, k)
                copy = pltpu.make_async_remote_copy(
                    src_ref=current[c].at[at_axis(left[c], axis, other)],
                    dst_ref=per_chunk[c][1][stage].at[k - 1],
                    send_sem=send_sem.at[c, stage, k - 1],
                    recv_sem=recv_sem.at[c, stage, k - 1],
                    device_id=(device,), device_id_type=MESH,
                )
                copy.start()
                copies.append(copy)
            flying[c] = copies

        def advance(c, stage):
            axis = orders[c][stage]
            for copy in flying[c]:
                copy.wait()
            landed = per_chunk[c][1][stage]
            own = current[c][at_axis(left[c], axis, coords[axis])].astype(jnp.float32)
            for k in range(factors[axis] - 1):
                own = own + landed[k].astype(jnp.float32)
            left[c] = [other for other in left[c] if other != axis]
            if stage == stages - 1:
                finished[c] = own
            else:
                current[c] = per_chunk[c][2][stage]
                current[c][...] = own.astype(jnp.bfloat16)
                launch(c, stage + 1)

        def finish():
            for stage in range(stages):
                for c in range(chunks):
                    if stage or c:
                        advance(c, stage)
            return jnp.concatenate(finished, axis=-1)

        def computed(c):
            launch(c, 0)
            if c == 1:
                advance(0, 0)

        return computed, finish

    def place(start_ref, first, value, column, span):
        blocks = value.shape[0] // seqs
        lead = start_ref.shape[:-2]
        flat = value.reshape(blocks, seqs, span).astype(jnp.bfloat16)
        inner = lead[1:]
        size = 1
        for factor in inner:
            size *= factor
        whole = blocks // size
        start_ref[pl.ds(first * whole, whole), ..., column] = flat.reshape((whole,) + inner + (seqs, span))

    tile = min(total_rows, 256)
    tiles = total_rows // tile
    span = 256
    mixed_per_tile = tile // seqs
    out_rows = out_weight_ref.shape[0]
    computed, finish = exchanger(exchanges[0])

    per_chunk = exchanges[0][0]
    begin = 0
    for c in range(chunks):
        @pl.loop(0, tiles * (widths[c] // span))
        def _(step):
            row = step // (widths[c] // span)
            column = pl.multiple_of(lax.rem(step, widths[c] // span) * span, span)
            left_side = mixed_ref[pl.ds(row * mixed_per_tile, mixed_per_tile)].astype(jnp.float32)
            left_side = left_side.reshape(tile, mixed_ref.shape[2])[:, :out_rows].astype(jnp.bfloat16)
            part = jnp.dot(
                left_side, out_weight_ref[:, pl.ds(pl.multiple_of(begin + column, span), span)],
                preferred_element_type=jnp.float32,
            )
            place(per_chunk[c][0], row, part, pl.ds(column, span), span)
        begin += widths[c]
        computed(c)

    projected = finish()
    settled = layer_norm(
        residual_scale * tokens_ref[...].astype(jnp.float32) + projected, gain_ref[0:1], bias_ref[0:1]
    )
    settled_ref[...] = settled

    mine = tuple(coords[axis] for axis in range(stages)[::-1])
    begin = 0
    for c in range(chunks):
        gathered[c][mine] = settled[:, begin:begin + widths[c]]
        begin += widths[c]
    flying = [None] * chunks
    have = [[] for _ in orders]

    def spread(c, stage):
        axis = orders[c][::-1][stage]
        index = tuple(
            slice(None) if other in have[c] else coords[other] for other in range(stages)[::-1]
        )
        copies = []
        for k in range(1, factors[axis]):
            _, device = partner(axis, k)
            copy = pltpu.make_async_remote_copy(
                src_ref=gathered[c].at[index], dst_ref=gathered[c].at[index],
                send_sem=gather_send.at[c, stage, k - 1], recv_sem=gather_recv.at[c, stage, k - 1],
                device_id=(device,), device_id_type=MESH,
            )
            copy.start()
            copies.append(copy)
        flying[c] = copies
        have[c].append(axis)

    for c in range(chunks):
        spread(c, 0)
    for stage in range(stages):
        for c in range(chunks):
            for copy in flying[c]:
                copy.wait()
            if stage < stages - 1:
                spread(c, stage + 1)
    begin = 0
    for c in range(chunks):
        block = gathered[c][...].astype(jnp.float32).reshape(total_rows, widths[c])
        rows_ref[:, begin:begin + widths[c]] = block.astype(jnp.bfloat16)
        begin += widths[c]

    for i in (0, 1, 3, 4):
        loads[i].wait()
    units = gate_ref.shape[1]
    unit_span = span if units % span == 0 else units

    def hidden_of(inputs, gates, ups, depth=0):
        contract = (((1,), (depth,)), ((), ()))
        gate_val = lax.dot_general(inputs, gates, contract, preferred_element_type=jnp.float32)
        up_val = lax.dot_general(inputs, ups, contract, preferred_element_type=jnp.float32)
        return (jax.nn.silu(gate_val) * up_val).astype(jnp.bfloat16)

    @pl.loop(0, tiles)
    def _(row):
        at_rows = pl.ds(pl.multiple_of(row * tile, tile), tile)
        dense_ref[at_rows, :] = hidden_of(
            rows_ref[at_rows, :], dense_gate_ref[...], dense_up_ref[...], 1
        )
        if unit_span == units:
            hidden_ref[at_rows, :] = hidden_of(rows_ref[at_rows, :], gate_ref[...], up_ref[...])
        else:
            @pl.loop(0, units // unit_span)
            def _(step):
                at_units = pl.ds(pl.multiple_of(step * unit_span, unit_span), unit_span)
                hidden_ref[at_rows, at_units] = hidden_of(
                    rows_ref[at_rows, :], gate_ref[:, at_units], up_ref[:, at_units]
                )

    for i in (2, 5):
        loads[i].wait()
    per_chunk = exchanges[1][0]
    computed, finish = exchanger(exchanges[1])
    begin = 0
    for c in range(chunks):
        @pl.loop(0, tiles * (widths[c] // span))
        def _(step):
            row = step // (widths[c] // span)
            column = pl.multiple_of(lax.rem(step, widths[c] // span) * span, span)
            at_columns = pl.ds(pl.multiple_of(begin + column, span), span)
            at_rows = pl.ds(pl.multiple_of(row * tile, tile), tile)
            expert_out = jnp.dot(
                hidden_ref[at_rows, :], down_ref[:, at_columns], preferred_element_type=jnp.float32
            )
            dense_out = jnp.dot(
                dense_ref[at_rows, :], dense_down_ref[:, at_columns], preferred_element_type=jnp.float32
            )
            part = share_ref[at_rows, :] * expert_out + scale_ref[:, at_columns] * dense_out
            place(per_chunk[c][0], row, part, pl.ds(column, span), span)
        begin += widths[c]
        computed(c)

    ffn = finish()
    result_ref[...] = layer_norm(
        residual_scale * settled_ref[...].astype(jnp.float32) + ffn, gain_ref[1:2], bias_ref[1:2]
    )


def whole_step(
    count, heads, tokens, gates, lengths, forget, norm_gain, norm_bias, dense_scale, routes, shares,
    query_weight, key_weight, value_weight, cache_keys, cache_values, out_weight,
    expert_gate, expert_up, expert_down, dense_gate, dense_up, dense_down,
):
    seqs, model = tokens.shape
    factors = factors_of(count)
    stages = len(factors)
    orders = orders_of(stages)
    narrow = model * 3 // 8
    widths = [model - narrow, narrow]
    total_rows = count * seqs
    lead = tuple(factors[::-1])
    scratch = [
        pltpu.VMEM(array.shape, array.dtype)
        for array in (expert_gate, expert_up, expert_down, dense_gate, dense_up, dense_down)
    ]
    scratch += [
        pltpu.SemaphoreType.DMA((6,)),
        *[
            pltpu.VMEM(array.shape, array.dtype)
            for array in (query_weight, key_weight, value_weight, cache_keys, cache_values, out_weight)
        ],
        pltpu.SemaphoreType.DMA((9,)),
        pltpu.VMEM((heads * seqs, key_weight.shape[1]), jnp.float32),
        pltpu.VMEM((total_rows, 128), jnp.float32),
        pltpu.VMEM((count, seqs, 128), jnp.bfloat16),
        pltpu.VMEM((total_rows, 1), jnp.float32),
        pltpu.VMEM((count, seqs, 128), jnp.bfloat16),
        pltpu.SemaphoreType.DMA((count - 1,)),
        pltpu.SemaphoreType.DMA((count - 1,)),
        pltpu.VMEM((total_rows, model), jnp.bfloat16),
        pltpu.VMEM((total_rows, expert_gate.shape[1]), jnp.bfloat16),
        pltpu.VMEM((total_rows, dense_gate.shape[0]), jnp.bfloat16),
        pltpu.VMEM((seqs, model), jnp.bfloat16),
    ]
    most = max(factors) - 1
    for _ in range(2):
        for order, width in zip(orders, widths):
            shapes = step_shapes(factors, order, seqs, width)
            scratch.append(pltpu.VMEM(lead + (seqs, width), jnp.bfloat16))
            scratch += [pltpu.VMEM(shape[0], jnp.bfloat16) for shape in shapes]
            scratch += [pltpu.VMEM(shape[1], jnp.bfloat16) for shape in shapes[:-1]]
        scratch += [pltpu.SemaphoreType.DMA((len(orders), stages, most))] * 2
    scratch += [pltpu.VMEM(lead + (seqs, width), jnp.bfloat16) for width in widths]
    scratch += [pltpu.SemaphoreType.DMA((len(orders), stages, most))] * 2
    vmem = pl.BlockSpec(memory_space=pltpu.VMEM)
    away = pl.BlockSpec(memory_space=pl.ANY)
    return pl.pallas_call(
        functools.partial(kernel, count, factors, orders, widths, heads),
        out_shape=jax.ShapeDtypeStruct((seqs, model), jnp.bfloat16),
        in_specs=[vmem] * 2
        + [pl.BlockSpec(memory_space=pltpu.SMEM)]
        + [vmem] * 6
        + [away] * 12,
        out_specs=vmem,
        scratch_shapes=scratch,
        compiler_params=pltpu.CompilerParams(
            collective_id=0, has_side_effects=True, vmem_limit_bytes=60 * 1024 * 1024
        ),
        name="whole_step",
    )(
        tokens, gates, lengths, forget, norm_gain, norm_bias, dense_scale, routes, shares,
        query_weight, key_weight, value_weight, cache_keys, cache_values, out_weight,
        expert_gate, expert_up, expert_down, dense_gate, dense_up, dense_down,
    )


def local(
    tokens,
    cache_keys,
    cache_values,
    cum_gates,
    lengths,
    query_weight,
    key_weight,
    value_weight,
    forget_weight,
    out_weight,
    norm_gain,
    norm_bias,
    dense_gate_weight,
    dense_up_weight,
    dense_down_weight,
    dense_scale,
    expert_gate_weight,
    expert_up_weight,
    expert_down_weight,
    routes,
    route_weights,
):
    count = lax.axis_size("ep")
    head_dim = key_weight.shape[1] // cum_gates.shape[2]
    heads = query_weight.shape[1] // head_dim
    return whole_step(
        count, heads, tokens, jnp.transpose(cum_gates, (0, 2, 1)), lengths, forget_weight.T,
        norm_gain, norm_bias, dense_scale[None, :], routes.T, route_weights.T,
        query_weight, key_weight, value_weight, cache_keys, cache_values, out_weight,
        expert_gate_weight, expert_up_weight, expert_down_weight,
        dense_gate_weight.T, dense_up_weight.T, dense_down_weight,
    )


def solution(mesh):
    return jax.shard_map(
        local,
        mesh=mesh,
        in_specs=(
            P("ep", None),
            P("ep", None, None),
            P("ep", None, None),
            P("ep", None, None),
            P("ep"),
            P(),
            P(),
            P(),
            P(),
            P("ep", None),
            P(),
            P(),
            P(None, "ep"),
            P(None, "ep"),
            P("ep", None),
            P(),
            P(None, "ep"),
            P(None, "ep"),
            P("ep", None),
            P(),
            P(),
        ),
        out_specs=P("ep", None),
        check_vma=False,
    )
```

profile of v0, /device:TPU:0, one launch (start us, length us, event | category | flops | bytes accessed | tf_op | source)
XLA Modules:
  0.0 143.0 jit_solution(14812548292037431368)
XLA Ops:
  0.0 0.0 copy-start
  0.0 4.0 %copy.22.gate_hbm = bf16[2048,448]{1,0:T(8,128)(2,1)} copy(bf16[2048,448]{0,1:T(8,128)(2,1)} %param.37) | data formatting | bytes 3670016 | tf_op args[16]
  4.0 0.0 copy-done
  4.0 2.5 %copy.23.up_hbm = bf16[2048,448]{1,0:T(8,128)(2,1)} copy(bf16[2048,448]{0,1:T(8,128)(2,1)S(1)} %copy-done) | data formatting | bytes 3670016 | tf_op args[17]
  6.4 135.2 %whole_step.1 = bf16[8,2048]{1,0:T(8,128)(2,1)} custom-call(bf16[8,2048]{1,0:T(8,128)(2,1)} %tokens_ref.1, f32[8,2,1024]{2,1,0:T(2,128)} %bitcast.9, s32[8]{0:T(128)} %lengths_ref.1, bf16[2,2048]{1,0:T(2,128)(2,1)} %bitcast.10, f32[2,2048]{1,0:T(2,128)} %gain_ref.1, f32[2,2048]{1,0:T(2,128)} %bias_ref.1, f32[1,2048]{1,0:T(1,128)} %bitcast.11, ...), custom_call_target="tpu_custom_call" | custom-call | tf_op jit(solution)/shard_map/whole_step/pallas_call | solution.py:499
  141.6 1.4 copy.25
Async XLA Ops:
  0.0 4.0 %copy-start = (bf16[2048,448]{0,1:T(8,128)(2,1)S(1)}, bf16[2048,448]{0,1:T(8,128)(2,1)}, u32[]{:S(2)}) copy-start(bf16[2048,448]{0,1:T(8,128)(2,1)} %param.38) | copy-start | bytes 5505028
where the time goes:
time: 143 us
  Pallas kernels  135 us (94%)
  local copies, waits for them, and re-layouts  7.8 us (5%)
    pallas_call x1, Pallas kernels, whole_step(): pl.pallas_call(functools.partial(kernel, count, factors, orders, widths,...  135 us
    unnamed x5, local copies, waits for them, and re-layouts  7.8 us

commit v1 on v0

v1 whole, which is shorter than its diff:
```python
import functools
import jax
import jax.numpy as jnp
from jax import lax
from jax.experimental import pallas as pl
from jax.experimental.pallas import tpu as pltpu
from jax.sharding import PartitionSpec as P

EXPERTS = 8
RING = 4
AXES = 3
MESH = pl.DeviceIdType.MESH

residual_scale = 1.4142135
norm_eps = 1e-05


def layer_norm(values, gain_row, shift_row):
    centre = jnp.mean(values, axis=-1, keepdims=True)
    centred = values - centre
    spread = jnp.mean(centred * centred, axis=-1, keepdims=True)
    return (centred * lax.rsqrt(spread + norm_eps) * gain_row + shift_row).astype(jnp.bfloat16)


def attend(
    heads, kv_count, tokens_ref, query_weight_ref, key_weight_ref, value_weight_ref,
    forget_ref, keys_ref, values_ref, gates_ref, lengths_ref, query_ref, rows_ref, waits,
):
    seqs, model = tokens_ref.shape
    width = key_weight_ref.shape[1]
    head_dim = width // kv_count
    grouped = heads // kv_count
    cache_len = keys_ref.shape[1]
    ratio_value = head_dim ** (-0.5)
    tokens = tokens_ref[...]
    wide = tokens.astype(jnp.float32)
    fresh_gate = jax.nn.log_sigmoid(
        jnp.concatenate(
            [
                jnp.sum(wide * forget_ref[j:j + 1, :].astype(jnp.float32), axis=1, keepdims=True)
                for j in range(kv_count)
            ],
            axis=1,
        )
    )
    waits["keys"]()
    fresh_key = jnp.dot(tokens, key_weight_ref[...], preferred_element_type=jnp.float32)
    fresh_key = fresh_key.astype(jnp.bfloat16).astype(jnp.float32)
    fresh_value = jnp.dot(tokens, value_weight_ref[...], preferred_element_type=jnp.float32)
    fresh_value = fresh_value.astype(jnp.bfloat16).astype(jnp.float32)
    pieces = waits["pieces"]
    piece = model // pieces
    for i in range(pieces):
        waits["query"](i)
        part = jnp.dot(
            tokens, query_weight_ref[:, i * piece:(i + 1) * piece], preferred_element_type=jnp.float32
        ).astype(jnp.bfloat16).astype(jnp.float32)
        for h in range(piece // head_dim):
            head = i * (piece // head_dim) + h
            group = head // grouped
            fields = [jnp.zeros((seqs, head_dim), jnp.float32)] * kv_count
            fields[group] = part[:, h * head_dim:(h + 1) * head_dim]
            query_ref[head * seqs:(head + 1) * seqs, :] = jnp.concatenate(fields, axis=1)
    waits["caches"]()
    positions = lax.broadcasted_iota(jnp.int32, (kv_count, cache_len), 1)
    row_group = lax.broadcasted_iota(jnp.int32, (heads, 1), 0) // grouped
    for b in range(seqs):
        length = lengths_ref[b]
        gates = gates_ref[b]
        latest = jnp.sum(jnp.where(positions == length - 1, gates, 0.0), axis=1, keepdims=True)
        offsets = jnp.where(positions < length, latest - gates, -jnp.inf)
        spread = offsets[0:1] + fresh_gate[b:b + 1, 0:1]
        spread = jnp.broadcast_to(spread, (heads, cache_len))
        for j in range(1, kv_count):
            spread = jnp.where(row_group == j, offsets[j:j + 1] + fresh_gate[b:b + 1, j:j + 1], spread)
        queries = query_ref[pl.ds(b, heads, stride=seqs), :]
        past = lax.dot_general(
            queries.astype(jnp.bfloat16), keys_ref[b], (((1,), (1,)), ((), ())),
            preferred_element_type=jnp.float32,
        )
        past = past * ratio_value + spread
        self_part = ratio_value * jnp.sum(queries * fresh_key[b:b + 1], axis=1, keepdims=True)
        highest = jnp.maximum(jnp.max(past, axis=1, keepdims=True), self_part)
        past_exp = jnp.exp(past - highest)
        own_exp = jnp.exp(self_part - highest)
        denominator = jnp.sum(past_exp, axis=1, keepdims=True) + own_exp
        past_weight = (past_exp / denominator).astype(jnp.bfloat16)
        own_weight = (own_exp / denominator).astype(jnp.bfloat16).astype(jnp.float32)
        mixed = jnp.dot(past_weight, values_ref[b], preferred_element_type=jnp.float32)
        mixed = mixed + own_weight * fresh_value[b:b + 1]
        rows_ref[pl.ds(b, heads, stride=seqs), :] = mixed
        waits["after"](b)
    fields = []
    for h in range(heads):
        group = h // grouped
        fields.append(rows_ref[h * seqs:(h + 1) * seqs, group * head_dim:(group + 1) * head_dim])
    return jnp.concatenate(fields, axis=1).astype(jnp.bfloat16)


def kernel(
    widths, heads,
    tokens_ref, gates_ref, lengths_ref, forget_ref, gain_ref, bias_ref, scale_ref,
    routes_ref, shares_ref, query_hbm, key_hbm, value_hbm, keys_hbm, values_hbm, out_hbm,
    gate_hbm, up_hbm, down_hbm, dense_gate_hbm, dense_up_hbm, dense_down_hbm,
    result_ref, *scratch,
):
    pool = list(scratch)
    take = lambda amount: [pool.pop(0) for _ in range(amount)]
    gate_ref, up_ref, down_ref, dense_gate_ref, dense_up_ref, dense_down_ref = take(6)
    load_sem, swap_send, swap_recv = take(3)
    query_weight_ref, key_weight_ref, value_weight_ref, keys_ref, values_ref, early_sem = take(6)
    query_ref, attended_rows_ref, share_ref, rows_ref, hidden_ref, dense_ref, settled_ref = take(7)
    dense_in_ref, dense_out_ref = take(2)
    slab_refs = take(2)
    slab_own, scatter_send, scatter_recv, slab_send, slab_recv, twin_send, twin_recv = take(7)
    queue_ref, queue_send, queue_recv, back_ref, back_in_ref, back_send, back_recv = take(7)
    chunks = len(widths)
    gathered = take(chunks)
    gather_send, gather_recv = take(2)
    per_chunk = []
    for _ in range(chunks):
        per_chunk.append((take(1)[0], take(AXES), take(AXES - 1)))
    reduce_send, reduce_recv = take(2)
    total_rows, model = rows_ref.shape
    seqs = tokens_ref.shape[0]
    slab = model // RING
    half = slab // 2

    me = lax.axis_index("ep")
    core = lax.rem(me, 2)
    twin = me + 1 - 2 * core
    coords, strides, rest, stride = [], [], me // 2, 2
    for _ in range(AXES):
        coords.append(lax.rem(rest, RING))
        strides.append(stride)
        rest = rest // RING
        stride *= RING
    x, y, z = coords

    def partner(axis, k):
        other = lax.rem(coords[axis] + k, RING)
        return other, me + (other - coords[axis]) * strides[axis]

    def remote(source, target, send, recv, device):
        return pltpu.make_async_remote_copy(
            src_ref=source, dst_ref=target, send_sem=send, recv_sem=recv,
            device_id=(device,), device_id_type=MESH,
        )

    barrier = pltpu.get_barrier_semaphore()
    pl.semaphore_signal(barrier, inc=1, device_id=(twin,), device_id_type=MESH)
    for axis in range(AXES):
        for k in range(1, RING):
            pl.semaphore_signal(
                barrier, inc=1, device_id=(partner(axis, k)[1],), device_id_type=MESH
            )

    pieces = 4
    piece = model // pieces
    early = [
        pltpu.make_async_copy(source, target, early_sem.at[i])
        for i, (source, target) in enumerate(
            [(key_hbm, key_weight_ref), (value_hbm, value_weight_ref)]
            + [
                (
                    query_hbm.at[:, pl.ds(i * piece, piece)],
                    query_weight_ref.at[:, pl.ds(i * piece, piece)],
                )
                for i in range(pieces)
            ]
            + [(keys_hbm, keys_ref), (values_hbm, values_ref)]
        )
    ]
    own_slabs = [
        pltpu.make_async_copy(
            out_hbm.at[:, pl.ds(pl.multiple_of(x * slab + c * half, half), half)],
            slab_refs[c].at[z, y, x, core], slab_own.at[c],
        )
        for c in range(2)
    ]
    for copy in own_slabs:
        copy.start()
    for copy in early:
        copy.start()
    pl.semaphore_wait(barrier, 1 + AXES * (RING - 1))

    scatter = []
    for k in range(1, RING):
        other, device = partner(0, k)
        for c in range(2):
            scatter.append(
                remote(
                    out_hbm.at[:, pl.ds(pl.multiple_of(other * slab + c * half, half), half)],
                    slab_refs[c].at[z, y, x, core],
                    scatter_send.at[c, k - 1], scatter_recv.at[c, k - 1], device,
                )
            )
    for copy in scatter:
        copy.start()

    sources = (gate_hbm, up_hbm, down_hbm, dense_gate_hbm, dense_up_hbm, dense_down_hbm)
    targets = (gate_ref, up_ref, down_ref, dense_gate_ref, dense_up_ref, dense_down_ref)
    loads = [
        pltpu.make_async_copy(source, target.at[0], load_sem.at[i])
        for i, (source, target) in enumerate(zip(sources, targets))
    ]
    swaps = [
        remote(source, target.at[1], swap_send.at[i], swap_recv.at[i], twin)
        for i, (source, target) in enumerate(zip(sources, targets))
    ]

    slab_orders = [[1, 2], [2, 1]]
    slab_have = [[], []]
    slab_flying = [[], []]
    twins = []

    def slab_at(c, fixed):
        at = [fixed.get(axis, slice(None)) for axis in (2, 1)]
        return slab_refs[c].at[at[0], at[1], :, core]

    def to_twin(c, number, block):
        copy = remote(block, block, twin_send.at[c, number], twin_recv.at[c, number], twin)
        copy.start()
        twins.append(copy)

    def slab_launch(c, stage):
        axis = slab_orders[c][stage]
        fixed = {other: coords[other] for other in (1, 2) if other not in slab_have[c]}
        copies = []
        for k in range(1, RING):
            copy = remote(
                slab_at(c, fixed), slab_at(c, fixed),
                slab_send.at[c, stage, k - 1], slab_recv.at[c, stage, k - 1], partner(axis, k)[1],
            )
            copy.start()
            copies.append(copy)
        slab_flying[c] = copies

    def slab_land(c, stage):
        axis = slab_orders[c][stage]
        for k, copy in enumerate(slab_flying[c], 1):
            copy.wait()
            fixed = {other: coords[other] for other in (1, 2) if other not in slab_have[c]}
            fixed[axis] = lax.rem(coords[axis] + RING - k, RING)
            to_twin(c, 1 + stage * (RING - 1) + k - 1, slab_at(c, fixed))
        slab_have[c].append(axis)

    def slabs_begin():
        for copy in own_slabs:
            copy.wait()
        for copy in scatter:
            copy.wait()
        for c in range(2):
            slab_launch(c, 0)
        for c in range(2):
            to_twin(c, 0, slab_at(c, {1: y, 2: z}))

    def slabs_second():
        for c in range(2):
            slab_land(c, 0)
            slab_launch(c, 1)

    def wait_all(some):
        for copy in some:
            copy.wait()

    def wait_query(i):
        early[2 + i].wait()
        if i == pieces - 1:
            slabs_begin()

    def wait_caches():
        for copy in loads + swaps:
            copy.start()
        wait_all(early[2 + pieces:])

    def after(b):
        if b == 1:
            slabs_second()

    waits = {
        "keys": lambda: wait_all(early[:2]),
        "query": wait_query,
        "pieces": pieces,
        "caches": wait_caches,
        "after": after,
    }
    kv_count = gates_ref.shape[1]
    attended = attend(
        heads, kv_count, tokens_ref, query_weight_ref, key_weight_ref, value_weight_ref,
        forget_ref, keys_ref, values_ref, gates_ref, lengths_ref, query_ref,
        attended_rows_ref, waits,
    )
    queue_ref[x] = attended
    queued = []
    for k in range(1, RING):
        copy = remote(
            queue_ref.at[x], queue_ref.at[x], queue_send.at[k - 1], queue_recv.at[k - 1],
            partner(0, k)[1],
        )
        copy.start()
        queued.append(copy)

    own_expert = me // (2 * RING ** AXES // EXPERTS)
    share_tile = 16 * seqs
    chosen = jnp.sum(
        jnp.where(routes_ref[...] == own_expert, shares_ref[...], 0.0), axis=0, keepdims=True
    )
    row = lax.broadcasted_iota(jnp.int32, (share_tile, 2 * share_tile), 0)
    lane = lax.broadcasted_iota(jnp.int32, (share_tile, 2 * share_tile), 1)
    wanted = lane == (row // seqs) * (2 * seqs) + core * seqs + lax.rem(row, seqs)
    for i in range(total_rows // share_tile):
        share_ref[i * share_tile:(i + 1) * share_tile, :] = jnp.sum(
            jnp.where(wanted, chosen[:, 2 * i * share_tile:2 * (i + 1) * share_tile], 0.0),
            axis=1, keepdims=True,
        )

    for c in range(2):
        slab_land(c, 1)
    wait_all(queued)
    wait_all(twins)
    lines = queue_ref[...].astype(jnp.float32).reshape(RING * seqs, model).astype(jnp.bfloat16)
    for c in range(2):
        part = jnp.dot(
            lines, slab_refs[c][...].reshape(model, half), preferred_element_type=jnp.float32
        )
        back_ref[:, :, c * half:(c + 1) * half] = part.reshape(RING, seqs, half)
    back_in_ref[x] = back_ref[x]
    returned = []
    for k in range(1, RING):
        other, device = partner(0, k)
        copy = remote(
            back_ref.at[other], back_in_ref.at[x], back_send.at[k - 1], back_recv.at[k - 1], device
        )
        copy.start()
        returned.append(copy)

    wait_all(loads)
    wait_all(swaps)
    units = dense_gate_ref.shape[1]
    pitch = (units + 15) // 16 * 16
    room = dense_out_ref.shape[0]
    gap = jnp.zeros((pitch - units, model), jnp.float32)
    rest = jnp.zeros((room - 2 * pitch, model), jnp.float32)

    def packed(ref):
        return jnp.concatenate(
            [ref[0].astype(jnp.float32), gap, ref[1].astype(jnp.float32), gap, rest], axis=0
        ).astype(jnp.bfloat16)

    dense_in_ref[:room, :] = packed(dense_gate_ref)
    dense_in_ref[room:, :] = packed(dense_up_ref)
    dense_out_ref[...] = packed(dense_down_ref)

    wait_all(returned)
    projected = jnp.concatenate([back_in_ref[i] for i in range(RING)], axis=1)
    settled = layer_norm(
        residual_scale * tokens_ref[...].astype(jnp.float32) + projected, gain_ref[0:1], bias_ref[0:1]
    )
    settled_ref[...] = settled

    orders = [[(c + stage) % AXES for stage in range(AXES)] for c in range(chunks)]
    begin = 0
    for c in range(chunks):
        gathered[c][z, y, x] = settled[:, begin:begin + widths[c]]
        begin += widths[c]
    flying = [None] * chunks
    have = [[] for _ in orders]

    def spread(c, stage):
        axis = orders[c][stage]
        index = tuple(
            slice(None) if other in have[c] else coords[other] for other in range(AXES)[::-1]
        )
        copies = []
        for k in range(1, RING):
            copy = remote(
                gathered[c].at[index], gathered[c].at[index],
                gather_send.at[c, stage, k - 1], gather_recv.at[c, stage, k - 1],
                partner(axis, k)[1],
            )
            copy.start()
            copies.append(copy)
        flying[c] = copies
        have[c].append(axis)

    for c in range(chunks):
        spread(c, 0)
    for stage in range(AXES):
        for c in range(chunks):
            wait_all(flying[c])
            if stage < AXES - 1:
                spread(c, stage + 1)
    begin = 0
    for c in range(chunks):
        block = gathered[c][...].astype(jnp.float32).reshape(total_rows, widths[c])
        rows_ref[:, begin:begin + widths[c]] = block.astype(jnp.bfloat16)
        begin += widths[c]

    tile = 256
    tiles = total_rows // tile
    span = 256
    contract = (((1,), (1,)), ((), ()))

    @pl.loop(0, tiles)
    def _(row):
        at_rows = pl.ds(pl.multiple_of(row * tile, tile), tile)
        inputs = rows_ref[at_rows, :]
        both = lax.dot_general(inputs, dense_in_ref[...], contract, preferred_element_type=jnp.float32)
        dense_ref[at_rows, :] = (jax.nn.silu(both[:, :room]) * both[:, room:]).astype(jnp.bfloat16)

        @pl.loop(0, 2)
        def _(side):
            gate_val = lax.dot_general(
                rows_ref[at_rows, :], gate_ref[side], contract, preferred_element_type=jnp.float32
            )
            up_val = lax.dot_general(
                rows_ref[at_rows, :], up_ref[side], contract, preferred_element_type=jnp.float32
            )
            hidden_ref[side, at_rows, :] = (jax.nn.silu(gate_val) * up_val).astype(jnp.bfloat16)

    def at_axis(left, axis, index):
        return tuple(index if other == axis else slice(None) for other in left)

    current = [entry[0] for entry in per_chunk]
    left = [list(range(AXES))[::-1] for _ in orders]
    sending = [None] * chunks
    finished = [None] * chunks

    def launch(c, stage):
        axis = orders[c][stage]
        copies = []
        for k in range(1, RING):
            other, device = partner(axis, k)
            copy = remote(
                current[c].at[at_axis(left[c], axis, other)], per_chunk[c][1][stage].at[k - 1],
                reduce_send.at[c, stage, k - 1], reduce_recv.at[c, stage, k - 1], device,
            )
            copy.start()
            copies.append(copy)
        sending[c] = copies

    def advance(c, stage):
        axis = orders[c][stage]
        wait_all(sending[c])
        landed = per_chunk[c][1][stage]
        own = current[c][at_axis(left[c], axis, coords[axis])].astype(jnp.float32)
        for k in range(RING - 1):
            own = own + landed[k].astype(jnp.float32)
        left[c] = [other for other in left[c] if other != axis]
        if stage == AXES - 1:
            finished[c] = own
        else:
            current[c] = per_chunk[c][2][stage]
            current[c][...] = own.astype(jnp.bfloat16)
            launch(c, stage + 1)

    tile_lead = tile // seqs // (RING * RING)
    begin = 0
    for c in range(chunks):
        span = 128 if widths[c] % 256 else 256
        steps = widths[c] // span

        @pl.loop(0, tiles * steps)
        def _(step):
            row = step // steps
            column = pl.multiple_of(lax.rem(step, steps) * span, span)
            at_columns = pl.ds(pl.multiple_of(begin + column, span), span)
            at_rows = pl.ds(pl.multiple_of(row * tile, tile), tile)
            expert_out = jnp.dot(
                hidden_ref[0, at_rows, :], down_ref[0, :, at_columns], preferred_element_type=jnp.float32
            ) + jnp.dot(
                hidden_ref[1, at_rows, :], down_ref[1, :, at_columns], preferred_element_type=jnp.float32
            )
            dense_out = jnp.dot(
                dense_ref[at_rows, :], dense_out_ref[:, at_columns], preferred_element_type=jnp.float32
            )
            part = share_ref[at_rows, :] * expert_out + scale_ref[:, at_columns] * dense_out
            per_chunk[c][0][pl.ds(row * tile_lead, tile_lead), :, :, :, pl.ds(column, span)] = part.reshape(
                tile_lead, RING, RING, seqs, span
            ).astype(jnp.bfloat16)

        begin += widths[c]
        launch(c, 0)

    for stage in range(AXES):
        for c in range(chunks):
            advance(c, stage)
    ffn = jnp.concatenate(finished, axis=-1)
    result_ref[...] = layer_norm(
        residual_scale * settled_ref[...].astype(jnp.float32) + ffn, gain_ref[1:2], bias_ref[1:2]
    )


def whole_step(
    heads, tokens, gates, lengths, forget, norm_gain, norm_bias, dense_scale, routes, shares,
    query_weight, key_weight, value_weight, cache_keys, cache_values, out_weight,
    expert_gate, expert_up, expert_down, dense_gate, dense_up, dense_down,
):
    seqs, model = tokens.shape
    widths = [768, 640, 640]
    chips = RING ** AXES
    total_rows = chips * seqs
    lead = (RING,) * AXES
    half = model // RING // 2
    bf16 = jnp.bfloat16
    dma = pltpu.SemaphoreType.DMA
    room = 128
    scratch = [
        pltpu.VMEM((2,) + array.shape, array.dtype)
        for array in (expert_gate, expert_up, expert_down, dense_gate, dense_up, dense_down)
    ]
    scratch += [dma((6,)), dma((6,)), dma((6,))]
    scratch += [
        pltpu.VMEM(array.shape, array.dtype)
        for array in (query_weight, key_weight, value_weight, cache_keys, cache_values)
    ]
    scratch += [
        dma((8,)),
        pltpu.VMEM((heads * seqs, key_weight.shape[1]), jnp.float32),
        pltpu.VMEM((heads * seqs, key_weight.shape[1]), jnp.float32),
        pltpu.VMEM((total_rows, 1), jnp.float32),
        pltpu.VMEM((total_rows, model), bf16),
        pltpu.VMEM((2, total_rows, expert_gate.shape[0]), bf16),
        pltpu.VMEM((total_rows, room), bf16),
        pltpu.VMEM((seqs, model), bf16),
        pltpu.VMEM((2 * room, model), bf16),
        pltpu.VMEM((room, model), bf16),
    ]
    scratch += [pltpu.VMEM((RING, RING, RING, 2, out_weight.shape[0], half), bf16)] * 2
    scratch += [
        dma((2,)), dma((2, RING - 1)), dma((2, RING - 1)),
        dma((2, 2, RING - 1)), dma((2, 2, RING - 1)), dma((2, 7)), dma((2, 7)),
        pltpu.VMEM((RING, seqs, model), bf16), dma((RING - 1,)), dma((RING - 1,)),
        pltpu.VMEM((RING, seqs, model // RING), jnp.float32),
        pltpu.VMEM((RING, seqs, model // RING), jnp.float32),
        dma((RING - 1,)), dma((RING - 1,)),
    ]
    scratch += [pltpu.VMEM(lead + (seqs, width), bf16) for width in widths]
    scratch += [dma((len(widths), AXES, RING - 1))] * 2
    for width in widths:
        scratch.append(pltpu.VMEM(lead + (seqs, width), bf16))
        scratch += [
            pltpu.VMEM((RING - 1,) + (RING,) * rest + (seqs, width), bf16) for rest in (2, 1, 0)
        ]
        scratch += [pltpu.VMEM((RING,) * rest + (seqs, width), bf16) for rest in (2, 1)]
    scratch += [dma((len(widths), AXES, RING - 1))] * 2
    vmem = pl.BlockSpec(memory_space=pltpu.VMEM)
    away = pl.BlockSpec(memory_space=pl.ANY)
    return pl.pallas_call(
        functools.partial(kernel, widths, heads),
        out_shape=jax.ShapeDtypeStruct((seqs, model), jnp.bfloat16),
        in_specs=[vmem] * 2
        + [pl.BlockSpec(memory_space=pltpu.SMEM)]
        + [vmem] * 6
        + [away] * 12,
        out_specs=vmem,
        scratch_shapes=scratch,
        compiler_params=pltpu.CompilerParams(
            collective_id=0, has_side_effects=True, vmem_limit_bytes=60 * 1024 * 1024
        ),
        name="whole_step",
    )(
        tokens, gates, lengths, forget, norm_gain, norm_bias, dense_scale, routes, shares,
        query_weight, key_weight, value_weight, cache_keys, cache_values, out_weight,
        expert_gate, expert_up, expert_down, dense_gate, dense_up, dense_down,
    )


def local(
    tokens,
    cache_keys,
    cache_values,
    cum_gates,
    lengths,
    query_weight,
    key_weight,
    value_weight,
    forget_weight,
    out_weight,
    norm_gain,
    norm_bias,
    dense_gate_weight,
    dense_up_weight,
    dense_down_weight,
    dense_scale,
    expert_gate_weight,
    expert_up_weight,
    expert_down_weight,
    routes,
    route_weights,
):
    head_dim = key_weight.shape[1] // cum_gates.shape[2]
    heads = query_weight.shape[1] // head_dim
    return whole_step(
        heads, tokens, jnp.transpose(cum_gates, (0, 2, 1)), lengths, forget_weight.T,
        norm_gain, norm_bias, dense_scale[None, :], routes.T, route_weights.T,
        query_weight, key_weight, value_weight, cache_keys, cache_values, out_weight,
        expert_gate_weight.T, expert_up_weight.T, expert_down_weight,
        dense_gate_weight.T, dense_up_weight.T, dense_down_weight,
    )


def solution(mesh):
    return jax.shard_map(
        local,
        mesh=mesh,
        in_specs=(
            P("ep", None),
            P("ep", None, None),
            P("ep", None, None),
            P("ep", None, None),
            P("ep"),
            P(),
            P(),
            P(),
            P(),
            P("ep", None),
            P(),
            P(),
            P(None, "ep"),
            P(None, "ep"),
            P("ep", None),
            P(),
            P(None, "ep"),
            P(None, "ep"),
            P("ep", None),
            P(),
            P(),
        ),
        out_specs=P("ep", None),
        check_vma=False,
    )
```

time: 143 us -> 81.3 us (0.57)
  Pallas kernels: 135 us -> 79.7 us
  local copies, waits for them, and re-layouts: 7.8 us -> 1.38 us
    pallas_call x1, Pallas kernels: 135 us -> 79.7 us  [whole_step(): pl.pallas_call(functools.partial(kernel, widths, heads), out_shape=jax.Sh...]
    unnamed x5 -> x1, local copies, waits for them, and re-layouts: 7.8 us -> 1.38 us
where the time goes in v1:
time: 81.3 us; the launch traced here: 81.1 us
  Pallas kernels  79.7 us (98%)
  local copies, waits for them, and re-layouts  1.38 us (2%)
    pallas_call x1, Pallas kernels, whole_step(): pl.pallas_call(functools.partial(kernel, widths, heads), out_shape=jax.Sh...  79.7 us

profile of v1, /device:TPU:0, one launch (start us, length us, event | category | flops | bytes accessed | tf_op | source)
XLA Modules:
  0.0 81.1 jit_solution(9058945034609301321)
XLA Ops:
  0.0 79.7 %whole_step.1 = bf16[8,2048]{1,0:T(8,128)(2,1)} custom-call(bf16[8,2048]{1,0:T(8,128)(2,1)} %tokens_ref.1, f32[8,2,1024]{2,1,0:T(2,128)} %bitcast.13, s32[8]{0:T(128)} %lengths_ref.1, bf16[2,2048]{1,0:T(2,128)(2,1)} %bitcast.14, f32[2,2048]{1,0:T(2,128)} %gain_ref.1, f32[2,2048]{1,0:T(2,128)} %bias_ref.1, f32[1,2048]{1,0:T(1,128)} %bitcast.15, ...), custom_call_target="tpu_custom_call" | custom-call | tf_op jit(solution)/shard_map/whole_step/pallas_call | solution.py:550
  79.7 1.4 %copy.23 = bf16[8,2048]{1,0:T(8,128)(2,1)} copy(bf16[8,2048]{1,0:T(8,128)(2,1)} %whole_step.1) | data formatting | bytes 65536
